TPU v7x, 32 devices: a whole 2x2x4 slice. The times are simulated.
32 devices in a mesh: fs: 8 (over z, x), tp: 4 (over y, core).
Axes of the slice: x: 2, y: 2, z: 4, core: 2. Of those that a mesh axis runs over, the one named last changes fastest.
Arguments:
- tokens: bfloat16 [3584, 2304], P('fs'), may hold values from -6 to 6
- norm_gain: float32 [2304], replicated, may hold values from 0.1 to 1.9
- gate_weight: bfloat16 [2304, 6144], P('fs', 'tp'), may hold values from -0.125 to 0.125
- up_weight: bfloat16 [2304, 6144], P('fs', 'tp'), may hold values from -0.125 to 0.125
- down_weight: bfloat16 [6144, 2304], P('tp', 'fs'), may hold values from -0.078125 to 0.078125
- branch_gain: float32 [2304], replicated, may hold values from 0.1 to 1.9
Outputs:
- result: bfloat16 [3584, 2304], P('fs')
All inputs are finite; a program needn't handle non-finite values.
Results may differ from a plain program's by a relative error of at most 0.014.
Values may be sent and summed in bfloat16 or wider, within the bound.
A program may use at most 64 MiB of HBM per device.

v0:
```python
import functools

import jax
import jax.numpy as jnp
from jax import lax
from jax.experimental import pallas as pl
from jax.experimental.pallas import tpu as pltpu
from jax.sharding import PartitionSpec as P

MESH = pl.DeviceIdType.MESH
epsilon = 1e-06
SUB = 3
LAG = 2


def complete(own_tokens, summed, branch_gain):
    branch_scale = lax.rsqrt(jnp.mean(summed * summed, axis=-1, keepdims=True) + epsilon)
    return (own_tokens.astype(jnp.float32) + summed * branch_scale * branch_gain).astype(
        jnp.bfloat16
    )


def normalize(tokens, norm_gain):
    widened = tokens.astype(jnp.float32)
    scale = lax.rsqrt(jnp.mean(widened * widened, axis=-1, keepdims=True) + epsilon)
    return (widened * scale * norm_gain).astype(jnp.bfloat16)


def plain(tokens, norm_gain, gate_weight, up_weight, down_weight, branch_gain):
    normed = normalize(tokens, norm_gain)
    gate_whole, up_whole = (
        lax.all_gather(gate_weight, "fs", axis=0, tiled=True),
        lax.all_gather(up_weight, "fs", axis=0, tiled=True),
    )
    gate_sum = jnp.dot(normed, gate_whole, preferred_element_type=jnp.float32)
    up_sum = jnp.dot(normed, up_whole, preferred_element_type=jnp.float32)
    hidden = (jax.nn.silu(gate_sum) * up_sum).astype(jnp.bfloat16)
    partial_value = jnp.dot(
        hidden,
        lax.all_gather(down_weight, "fs", axis=1, tiled=True),
        preferred_element_type=jnp.float32,
    )
    summed = lax.psum(partial_value.astype(jnp.bfloat16), "tp").astype(jnp.float32)
    return complete(tokens, summed, branch_gain)


def log2(n):
    return n.bit_length() - 1


def kernel(n_fs, n_tp, group, tokens_ref, gate_ref, up_ref, down_ref, gain_ref, out_ref, *scratch):
    n_group = n_fs // group
    stages = log2(group * n_tp)
    tp_bits = log2(n_tp)
    xs, xn, wg, wu, wd, hid, gated = scratch[:7]
    held = scratch[7:7 + stages]
    arrived = scratch[7 + stages:7 + 2 * stages]
    (loc_sem, w_send, w_recv, x_send, x_recv, y_send, y_recv, r_send, r_recv, o_send, o_recv) = scratch[7 + 2 * stages:]
    f, t = lax.axis_index("fs"), lax.axis_index("tp")
    g, q = f // group, f % group
    rank = q * n_tp + t
    depth, width = gate_ref.shape[0], wg.shape[1]
    chunks, rq, cw = arrived[0].shape[0], *arrived[0].shape[2:]
    rows = n_tp * rq

    barrier = pltpu.get_barrier_semaphore()
    for k in range(1, n_fs):
        pl.semaphore_signal(barrier, inc=1, device_id=((f + k) % n_fs, t), device_id_type=MESH)
    for k in range(1, n_tp):
        pl.semaphore_signal(barrier, inc=1, device_id=(f, (t + k) % n_tp), device_id_type=MESH)

    at = pl.ds(pl.multiple_of(f * depth, depth), depth)
    mine = pl.ds(pl.multiple_of(q * width, width), width)
    local = [
        pltpu.make_async_copy(tokens_ref, xs.at[q], loc_sem.at[0]),
        pltpu.make_async_copy(gate_ref.at[:, mine], wg.at[at], loc_sem.at[1]),
        pltpu.make_async_copy(up_ref.at[:, mine], wu.at[at], loc_sem.at[2]),
        pltpu.make_async_copy(down_ref.at[:, mine], wd.at[at], loc_sem.at[3]),
    ]
    for copy in local:
        copy.start()
    pl.semaphore_wait(barrier, n_fs + n_tp - 2)

    first = {}
    for k in range(1, group):
        first[k] = pltpu.make_async_remote_copy(
            tokens_ref.at[t], xs.at[q, t], x_send.at[k], x_recv.at[k],
            device_id=(g * group + (q + k) % group, t), device_id_type=MESH,
        )
        first[k].start()
    moved = {}
    for a, (src, dst) in enumerate(((gate_ref, wg), (up_ref, wu), (down_ref, wd))):
        for dg in reversed(range(n_group)) if a < 2 else range(n_group):
            for dq in range(group):
                if dg + dq > 0:
                    to_q = (q + dq) % group
                    part = pl.ds(pl.multiple_of(to_q * width, width), width)
                    moved[a, dg, dq] = pltpu.make_async_remote_copy(
                        src.at[:, part], dst.at[at],
                        w_send.at[a, dg * group + dq], w_recv.at[a, dg * group + dq],
                        device_id=(((g + dg) % n_group) * group + to_q, t), device_id_type=MESH,
                    )
                    moved[a, dg, dq].start()
    def normalize_piece(block, piece):
        def strip(r, carry):
            at_rows = pl.ds(pl.multiple_of(r * 16, 16), 16)
            x = xs[block, piece, at_rows, :].astype(jnp.float32)
            scale = lax.rsqrt(jnp.mean(x * x, axis=-1, keepdims=True) + epsilon)
            xn[block, piece, at_rows, :] = (x * scale * gain_ref[...]).astype(jnp.bfloat16)
            return carry

        lax.fori_loop(0, rq // 16, strip, 0)

    for copy in local:
        copy.wait()
    for piece in range(n_tp):
        normalize_piece(q, piece)
    def spread(k, s):
        of = (q + group - k) % group
        bit = (t // 2**s) % 2
        copies = []
        for h in range(2 ** (tp_bits - 1 - s)):
            piece = xs.at[of, h * 2 ** (s + 1) + t % 2 ** (s + 1)]
            copies.append(pltpu.make_async_remote_copy(
                piece, piece, y_send.at[k, s, h], y_recv.at[k, s, h],
                device_id=(f, t + (1 - 2 * bit) * 2**s), device_id_type=MESH,
            ))
        return copies

    for k in range(1, group):
        first[k].wait_recv()
        for copy in spread(k, tp_bits - 1):
            copy.start()
        normalize_piece((q + group - k) % group, t)
    for s in reversed(range(tp_bits)):
        other = (t % 2 ** (s + 1) + 2**s) % 2 ** (s + 1)
        for k in range(1, group):
            for copy in spread(k, s):
                copy.wait_recv()
            if s > 0:
                for copy in spread(k, s - 1):
                    copy.start()
            for h in range(2 ** (tp_bits - 1 - s)):
                normalize_piece((q + group - k) % group, h * 2 ** (s + 1) + other)

    def arrived_weight(a):
        for (b, _, _), copy in moved.items():
            if a == b:
                copy.wait_recv()

    def gate_block(b, carry):
        x = xn[b].reshape(rows, xn.shape[-1])
        gate = jnp.dot(x, wg[...], preferred_element_type=jnp.float32)
        gated[b] = gate / (1.0 + jnp.exp(-gate))
        return carry

    def up_block(b, carry):
        x = xn[b].reshape(rows, xn.shape[-1])
        up = jnp.dot(x, wu[...], preferred_element_type=jnp.float32)
        hid[b] = (gated[b] * up).astype(jnp.bfloat16)
        return carry

    arrived_weight(0)
    lax.fori_loop(0, group, gate_block, 0)
    arrived_weight(1)
    lax.fori_loop(0, group, up_block, 0)

    def column(i):
        return ((g + i // SUB) % n_group) * SUB + i % SUB

    def order(i):
        rest = list(range(1, stages))
        turn = i % SUB % len(rest)
        return [0] + rest[turn:] + rest[:turn]

    def reduction(i, s):
        b = order(i)[s]
        bit = (rank // 2**b) % 2
        flip = 1 - 2 * bit
        if b < tp_bits:
            to = (f, t + flip * 2**b)
        else:
            to = (f + flip * 2 ** (b - tp_bits), t)
        return pltpu.make_async_remote_copy(
            held[s].at[i, :, 1 - bit], arrived[s].at[i], r_send.at[i, s], r_recv.at[i, s],
            device_id=to, device_id_type=MESH,
        )

    def columns(i):
        return pl.ds(pl.multiple_of(column(i) * cw, cw), cw)

    def down_chunk(i):
        def block(b, carry):
            part = lax.dot_general(
                hid[b], wd[columns(i), :], (((1,), (1,)), ((), ())),
                preferred_element_type=jnp.float32,
            ).astype(jnp.bfloat16)
            for piece in range(n_tp):
                owner = b * n_tp + piece
                place = sum((owner // 2**o) % 2 * 2**s for s, o in enumerate(order(i)))
                held[0][i, place // 2, place % 2] = part[piece * rq:(piece + 1) * rq]
            return carry

        lax.fori_loop(0, group, block, 0)

    def add_stage(i, s):
        reduction(i, s).wait_recv()
        bit = (rank // 2 ** order(i)[s]) % 2
        if s == stages - 1:
            total = held[s][i, 0, bit].astype(jnp.float32) + arrived[s][i, 0].astype(jnp.float32)
            out_ref[0, t, :, columns(i)] = total.astype(jnp.bfloat16)
            return

        def one(j, carry):
            total = held[s][i, j, bit].astype(jnp.float32) + arrived[s][i, j].astype(jnp.float32)
            held[s + 1][i, j // 2, j % 2] = total.astype(jnp.bfloat16)
            return carry

        lax.fori_loop(0, held[s].shape[1], one, 0)

    def sharing(i, s):
        bit = (t // 2**s) % 2
        copies = []
        for h in range(2 ** (tp_bits - 1 - s)):
            piece = out_ref.at[0, h * 2 ** (s + 1) + t % 2 ** (s + 1), :, columns(i)]
            copies.append(pltpu.make_async_remote_copy(
                piece, piece, o_send.at[i, s, h], o_recv.at[i, s, h],
                device_id=(f, t + (1 - 2 * bit) * 2**s), device_id_type=MESH,
            ))
        return copies

    def begin(part):
        dg = (n_group - part) % n_group
        for dq in range(group):
            if dg + dq > 0:
                moved[2, dg, dq].wait_recv()
        for i in range(part * SUB, (part + 1) * SUB):
            down_chunk(i)
            reduction(i, 0).start()

    def advance(part, s):
        for i in range(part * SUB, (part + 1) * SUB):
            add_stage(i, s)
            if s + 1 < stages:
                reduction(i, s + 1).start()
            else:
                for copy in sharing(i, tp_bits - 1):
                    copy.start()

    def share(part, s):
        for i in range(part * SUB, (part + 1) * SUB):
            for copy in sharing(i, s):
                copy.wait_recv()
            if s > 0:
                for copy in sharing(i, s - 1):
                    copy.start()

    total_steps = 1 + stages + tp_bits
    for slot in range(total_steps + LAG * (n_group - 1)):
        for part in reversed(range(n_group)):
            step = slot - LAG * part
            if step == 0:
                begin(part)
            elif 1 <= step <= stages:
                advance(part, step - 1)
            elif stages < step < total_steps:
                share(part, tp_bits - 1 - (step - 1 - stages))

    for copy in list(first.values()) + list(moved.values()):
        copy.wait_send()
    for k in range(1, group):
        for s in range(tp_bits):
            for copy in spread(k, s):
                copy.wait_send()
    for i in range(chunks):
        for s in range(stages):
            reduction(i, s).wait_send()
        for s in range(tp_bits):
            for copy in sharing(i, s):
                copy.wait_send()


def fused(n_fs, n_tp, group, tokens, norm_gain, gate_weight, up_weight, down_weight, branch_gain):
    rows, d = tokens.shape
    rq = rows // n_tp
    depth, hidden = gate_weight.shape
    width = hidden // group
    chunks = (n_fs // group) * SUB
    cw = d // chunks
    pieces = group * n_tp
    stages = log2(pieces)
    bf16, dma = jnp.bfloat16, pltpu.SemaphoreType.DMA
    hbm = pl.BlockSpec(memory_space=pl.ANY)
    vmem = pl.BlockSpec(memory_space=pltpu.VMEM)
    out = pl.pallas_call(
        functools.partial(kernel, n_fs, n_tp, group),
        out_shape=jax.ShapeDtypeStruct((1, n_tp, rq, d), bf16),
        in_specs=[hbm] * 4 + [vmem],
        out_specs=vmem,
        scratch_shapes=[
            pltpu.VMEM((group, n_tp, rq, d), bf16),
            pltpu.VMEM((group, n_tp, rq, d), bf16),
            pltpu.VMEM((d, width), bf16),
            pltpu.VMEM((d, width), bf16),
            pltpu.VMEM((d, width), bf16),
            pltpu.VMEM((group, rows, width), bf16),
            pltpu.VMEM((group, rows, width), jnp.float32),
        ]
        + [pltpu.VMEM((chunks, pieces >> (s + 1), 2, rq, cw), bf16) for s in range(stages)]
        + [pltpu.VMEM((chunks, pieces >> (s + 1), rq, cw), bf16) for s in range(stages)]
        + [
            dma((4,)),
            dma((3, n_fs)), dma((3, n_fs)),
            dma((group,)), dma((group,)),
            dma((group, log2(n_tp), n_tp)), dma((group, log2(n_tp), n_tp)),
            dma((chunks, stages)), dma((chunks, stages)),
            dma((chunks, log2(n_tp), n_tp)), dma((chunks, log2(n_tp), n_tp)),
        ],
        compiler_params=pltpu.CompilerParams(
            collective_id=0, has_side_effects=True, vmem_limit_bytes=60 * 1024 * 1024
        ),
    )(
        tokens.reshape(n_tp, rq, d), gate_weight, up_weight, down_weight.T, norm_gain.reshape(1, d),
    )
    return complete(tokens, out.reshape(rows, d).astype(jnp.float32), branch_gain)


def solution(mesh):
    n_fs, n_tp = mesh.shape["fs"], mesh.shape["tp"]

    def per_device(*args):
        tokens, _, gate_weight = args[:3]
        rows, d = tokens.shape
        depth, hidden = gate_weight.shape
        group = 4
        fits = (
            n_fs % group == 0
            and n_tp & (n_tp - 1) == 0
            and n_tp > 1
            and rows % (16 * n_tp) == 0
            and depth % 16 == 0
            and hidden % (128 * group) == 0
            and d % (128 * SUB * max(n_fs // group, 1)) == 0
        )
        if fits:
            return fused(n_fs, n_tp, group, *args)
        return plain(*args)

    in_specs = (P("fs", None), P(), P("fs", "tp"), P("fs", "tp"), P("tp", "fs"), P())
    return jax.shard_map(
        per_device, mesh=mesh, in_specs=in_specs, out_specs=P("fs", None), check_vma=False
    )
```

profile of v0, /device:TPU:0, one launch (start us, length us, event | category | flops | bytes accessed | tf_op | source)
XLA Modules:
  0.0 178.9 jit_solution(8898102910942326204)
XLA Ops:
  0.0 1.3 reshape.28.gain_ref
  1.3 0.0 copy-start.1
  1.3 171.4 %shard_map.64 = bf16[1,4,112,2304]{3,2,1,0:T(8,128)(2,1)} custom-call(bf16[4,112,2304]{2,1,0:T(8,128)(2,1)} %bitcast.10, bf16[288,1536]{1,0:T(8,128)(2,1)} %gate_ref.1, bf16[288,1536]{1,0:T(8,128)(2,1)} %up_ref.1, bf16[288,1536]{1,0:T(8,128)(2,1)} %bitcast.11, f32[1,2304]{1,0:T(1,128)} %reshape.28.gain_ref), custom_call_target="tpu_custom_call" | custom-call | tf_op jit(solution)/shard_map/pallas_call | solution.py:295
  172.7 0.0 copy-start
  172.8 2.2 %multiply_reduce_fusion = f32[4,112]{1,0:T(4,128)S(1)} fusion(bf16[1,4,112,2304]{3,2,1,0:T(8,128)(2,1)} %shard_map.64), kind=kLoop, calls=%fused_computation.4 | loop fusion | flops 3096128 | bytes 2066176 | tf_op jit(solution)/shard_map/reduce_sum | solution.py:17
  175.0 0.1 rsqrt.12
  175.1 0.0 copy-done.1
  175.1 0.0 copy-done
  175.1 3.8 %fusion.2 = bf16[448,2304]{1,0:T(8,128)(2,1)} fusion(bf16[448,2304]{1,0:T(8,128)(2,1)} %param.6, f32[2304]{0:T(1024)S(1)} %copy-done.1, f32[448]{0:T(512)S(1)} %rsqrt.12, bf16[1,4,112,2304]{3,2,1,0:T(8,128)(2,1)S(1)} %copy-done), kind=kLoop, calls=%fused_computation.3 | loop fusion | flops 6193152 | bytes 6204160 | tf_op jit(solution)/shard_map/convert_element_type | solution.py:18
  (1 shorter events, 0.0 us)
Async XLA Ops:
  1.3 173.8 %copy-start.1 = (f32[2304]{0:T(1024)S(1)}, f32[2304]{0:T(1024)}, u32[]{:S(2)}) copy-start(f32[2304]{0:T(1024)} %param.11) | copy-start | bytes 27652
  172.7 2.3 %copy-start = (bf16[1,4,112,2304]{3,2,1,0:T(8,128)(2,1)S(1)}, bf16[1,4,112,2304]{3,2,1,0:T(8,128)(2,1)}, u32[]{:S(2)}) copy-start(bf16[1,4,112,2304]{3,2,1,0:T(8,128)(2,1)} %shard_map.64) | copy-start | bytes 6193156
where the time goes:
time: 179 us
  Pallas kernels  171 us (96%)
  other arithmetic  6 us (3%)
    pallas_call x1, Pallas kernels, fused(): pl.pallas_call(functools.partial(kernel, n_fs, n_tp, group), out_shape=ja...  171 us
    convert_element_type x1, other arithmetic, complete(): (own_tokens.astype(jnp.float32) + summed * branch_scale * branch_gain).as...  3.78 us

commit v1 on v0

v1 whole, which is shorter than its diff:
```python
import functools

import jax
import jax.numpy as jnp
from jax import lax
from jax.experimental import pallas as pl
from jax.experimental.pallas import tpu as pltpu
from jax.sharding import PartitionSpec as P

MESH = pl.DeviceIdType.MESH
epsilon = 1e-06
GATE, UP, DOWN = 0, 1, 2
SUB = 3
STRIP = 16


def complete(own_tokens, summed, branch_gain):
    branch_scale = lax.rsqrt(jnp.mean(summed * summed, axis=-1, keepdims=True) + epsilon)
    return (own_tokens.astype(jnp.float32) + summed * branch_scale * branch_gain).astype(
        jnp.bfloat16
    )


def normalize(tokens, norm_gain):
    widened = tokens.astype(jnp.float32)
    scale = lax.rsqrt(jnp.mean(widened * widened, axis=-1, keepdims=True) + epsilon)
    return (widened * scale * norm_gain).astype(jnp.bfloat16)


def plain(tokens, norm_gain, gate_weight, up_weight, down_weight, branch_gain):
    normed = normalize(tokens, norm_gain)
    gate_whole, up_whole = (
        lax.all_gather(gate_weight, "fs", axis=0, tiled=True),
        lax.all_gather(up_weight, "fs", axis=0, tiled=True),
    )
    gate_sum = jnp.dot(normed, gate_whole, preferred_element_type=jnp.float32)
    up_sum = jnp.dot(normed, up_whole, preferred_element_type=jnp.float32)
    hidden = (jax.nn.silu(gate_sum) * up_sum).astype(jnp.bfloat16)
    partial_value = jnp.dot(
        hidden,
        lax.all_gather(down_weight, "fs", axis=1, tiled=True),
        preferred_element_type=jnp.float32,
    )
    summed = lax.psum(partial_value.astype(jnp.bfloat16), "tp").astype(jnp.float32)
    return complete(tokens, summed, branch_gain)


def kernel(tokens_ref, gate_ref, up_ref, down_ref, gain_ref, out_ref, *scratch):
    xs, xn, wg, wu, wd, gated, hid, part, pc, sm, r_end, r_mid, r_fin = scratch[:13]
    (loc_sem, z_send, z_recv, x_send, x_recv, y_send, y_recv, dx_send, dx_recv, dy_send, dy_recv,
     t_send, t_recv, td_send, td_recv, c_send, c_recv, e_send, e_recv, m_send, m_recv, f_send, f_recv,
     o_send, o_recv) = scratch[13:]
    f, t = lax.axis_index("fs"), lax.axis_index("tp")
    z, x, y, c = f // 2, f % 2, t // 2, t % 2
    h = z // 2
    middling = (z % 2 + z // 2) % 2
    is_mid, is_end = middling == 1, middling == 0
    plane = [z, z + 1 - 2 * (z % 2), 2 - h, 3 - 3 * h]
    slot = [0, 1, 3 - middling, 3 - middling]
    depth, width = gate_ref.shape[0], wg.shape[1] // 2
    rq, d = xn.shape[2:]
    strips = rq // STRIP
    chunks, cw = part.shape[0], part.shape[-1]
    rows = 8 * rq
    weights, inputs = (wg, wu, wd), (gate_ref, up_ref, down_ref)

    x_to, y_to, c_to = (f + 1 - 2 * x, t), (f, (t + 2) % 4), (f, t + 1 - 2 * c)
    yc_to = (f, (1 - y) * 2 + 1 - c)

    def z_to(k):
        return (plane[k] * 2 + x, t)

    barrier = pltpu.get_barrier_semaphore()
    for peer in (x_to, y_to, c_to, yc_to, z_to(1), z_to(2), z_to(3)):
        pl.semaphore_signal(barrier, inc=1, device_id=peer, device_id_type=MESH)

    def remote(src, dst, send, recv, to):
        return pltpu.make_async_remote_copy(
            src, dst, send, recv, device_id=to, device_id_type=MESH
        )

    def block(a, k, yy, lo=0, n=depth, flip=0):
        ff = plane[k] * 2 + (1 - x if flip else x)
        at = pl.ds(pl.multiple_of(ff * depth + lo, STRIP), n)
        return weights[a].at[at, pl.ds(pl.multiple_of(yy * width, width), width)]

    def quarter(a, k):
        return inputs[a].at[:, pl.ds(pl.multiple_of(plane[k] * width, width), width)]

    local = [pltpu.make_async_copy(tokens_ref.at[t], xs, loc_sem.at[3])] + [
        pltpu.make_async_copy(quarter(a, 0), block(a, 0, y), loc_sem.at[a]) for a in range(3)
    ]
    for copy in local:
        copy.start()

    sent = []
    sent_end, sent_mid = [], []

    def start(copy):
        copy.start()
        sent.append(copy)

    def start_end(copy):
        pl.when(is_end)(copy.start)
        sent_end.append(copy)

    def start_mid(copy):
        pl.when(is_mid)(copy.start)
        sent_mid.append(copy)

    def z_copy(a, k):
        return remote(
            quarter(a, k), block(a, 0, y), z_send.at[a, k], z_recv.at[a, slot[k]], z_to(k)
        )

    def z_wait(a, k):
        piece = block(a, k, y)
        remote(piece, piece, z_send.at[a, k], z_recv.at[a, k], z_to(k)).wait_recv()

    def across(a, k):
        src = quarter(a, 0) if k == 0 else block(a, k, y)
        return (
            remote(src, block(a, k, y), x_send.at[a, k], x_recv.at[a, k], x_to),
            remote(src, block(a, k, y), y_send.at[a, k], y_recv.at[a, k], y_to),
        )

    def diagonal(a, k):
        n = depth // 2
        first, second = block(a, k, y, 0, n, 1), block(a, k, 1 - y, n, n)
        return (
            remote(first, first, dy_send.at[a, k], dy_recv.at[a, k], y_to),
            remote(second, second, dx_send.at[a, k], dx_recv.at[a, k], x_to),
        )

    def spread(a, k):
        if k > 0:
            z_wait(a, k)
        for copy in across(a, k):
            start(copy)

    def relay(a, k):
        for got, on in zip(across(a, k), diagonal(a, k)):
            got.wait_recv()
            start(on)

    def settle(a, k):
        for got in diagonal(a, k):
            got.wait_recv()

    def strip(k, s):
        return xn.at[plane[k], c, pl.ds(s * STRIP, STRIP)]

    def token_copy(lane, k, s, to, slot):
        piece = strip(k, s)
        return remote(piece, piece, t_send.at[lane, s], t_recv.at[slot, s], to)

    def token_wait(k, s):
        token_copy(0, k, s, z_to(1), k).wait_recv()

    def token_pair(k):
        piece = xn.at[plane[k], c]
        return remote(piece, piece, td_send.at[k], td_recv.at[k], c_to)

    def token_relay(k, lane, to, slot, lo=0, hi=strips):
        for s in range(lo, hi):
            pl.when(is_mid)(lambda s=s: token_wait(k, s))
            start_mid(token_copy(lane, k, s, z_to(to), slot))
        if hi == strips:
            start_mid(token_pair(k))

    def token_take(k):
        for s in range(strips):
            pl.when(is_end)(lambda s=s: token_wait(k, s))
        start_end(token_pair(k))

    def from_near():
        token_relay(1, 2, 2, 3)

    def from_mid(lo=0, hi=strips):
        token_relay(2, 3, 1, 2, lo, hi)

    def from_far(lo=0, hi=strips):
        token_relay(3, 4, 1, 3, lo, hi)

    def token_settle(*which):
        for k in which:
            token_pair(k).wait_recv()

    pl.semaphore_wait(barrier, 7)

    def sends(role, pairs):
        for a, k in pairs:
            role(z_copy(a, k))

    sends(start_end, [(GATE, 1), (GATE, 2), (GATE, 3), (UP, 1), (UP, 2), (UP, 3)])
    sends(start_mid, [(GATE, 2), (GATE, 1), (GATE, 3), (UP, 2), (UP, 1), (UP, 3)])
    spread(GATE, 0)
    spread(UP, 0)

    local[0].wait()
    for s in range(strips):
        at_rows = pl.ds(s * STRIP, STRIP)
        v = xs[at_rows, :].astype(jnp.float32)
        scale = lax.rsqrt(jnp.mean(v * v, axis=-1, keepdims=True) + epsilon)
        xn[z, c, at_rows, :] = (v * scale * gain_ref[...]).astype(jnp.bfloat16)
    for s in range(strips):
        start(token_copy(0, 0, s, z_to(1), 1))
        start_mid(token_copy(1, 0, s, z_to(2), 2))
    start(token_pair(0))
    sends(start_end, [(DOWN, 1)])

    def product(w, zb, nb, n0, nw):
        v = xn[pl.ds(zb, nb)].reshape(nb * 2 * rq, d)
        return jnp.dot(
            v, w[:, pl.ds(pl.multiple_of(n0, nw), nw)], preferred_element_type=jnp.float32
        )

    def gate_rows(zb, nb):
        def one(i, carry):
            n0 = pl.multiple_of(i * width, width)
            v = product(wg, zb, nb, n0, width)
            v = v / (1.0 + jnp.exp(-v))
            gated[pl.ds(zb, nb), :, pl.ds(n0, width)] = v.reshape(nb, 2 * rq, width)
            return carry

        lax.fori_loop(0, 2, one, 0)

    def up_rows(zb, nb):
        def one(i, carry):
            n0 = pl.multiple_of(i * width, width)
            v = product(wu, zb, nb, n0, width).reshape(nb, 2 * rq, width)
            v = gated[pl.ds(zb, nb), :, pl.ds(n0, width)] * v
            hid[pl.ds(zb, nb), :, pl.ds(n0, width)] = v.astype(jnp.bfloat16)
            return carry

        lax.fori_loop(0, 2, one, 0)

    relay(GATE, 0)
    spread(GATE, 1)
    relay(UP, 0)
    spread(GATE, 2)
    relay(GATE, 1)
    spread(GATE, 3)
    spread(UP, 1)
    relay(GATE, 2)
    spread(UP, 2)
    relay(GATE, 3)
    relay(UP, 1)
    spread(UP, 3)
    spread(DOWN, 0)
    from_near()
    sends(start_mid, [(DOWN, 2), (DOWN, 3)])
    from_mid(0, 4)
    relay(UP, 2)
    for copy in local[1:]:
        copy.wait()
    for k in range(4):
        settle(GATE, k)
    token_take(1)
    token_settle(0, 1)
    gate_rows(h * 2, 2)
    from_mid(4)
    sends(start_mid, [(DOWN, 1)])
    relay(UP, 3)
    from_far(0, 4)
    token_take(2)
    token_settle(2)
    gate_rows(plane[2], 1)
    from_far(4)
    sends(start_end, [(DOWN, 2), (DOWN, 3)])
    spread(DOWN, 1)
    for k in range(4):
        settle(UP, k)
    up_rows(h * 2, 2)
    up_rows(plane[2], 1)
    relay(DOWN, 0)
    relay(DOWN, 1)
    token_take(3)
    token_settle(3)
    gate_rows(plane[3], 1)
    up_rows(plane[3], 1)

    def column(i):
        first = SUB - 1 - i if i < SUB else i
        return h * (chunks - 1) + (1 - 2 * h) * first

    def pair_copy(i):
        j = column(i)
        return remote(part.at[j, :, 1 - c], pc.at[j], c_send.at[j], c_recv.at[j], c_to)

    def down_chunk(i):
        j = column(i)
        value = lax.dot_general(
            hid[...].reshape(rows, 2 * width), wd[pl.ds(pl.multiple_of(j * cw, cw), cw), :], (((1,), (1,)), ((), ())),
            preferred_element_type=jnp.float32,
        ).astype(jnp.bfloat16)
        for zz in range(4):
            for cc in range(2):
                at = (zz * 2 + cc) * rq
                part[j, zz, cc] = value[at:at + rq]
        start(pair_copy(i))

    def add(*terms):
        return functools.reduce(lambda a, b: a + b, [v.astype(jnp.float32) for v in terms])

    def end_copies(i):
        j = column(i)
        return (
            remote(sm.at[j, pl.ds(2, 2)], r_end.at[j, pl.ds(1, 2)], e_send.at[j, 0], e_recv.at[j, 0], z_to(1)),
            remote(sm.at[j, 1], r_end.at[j, 0], e_send.at[j, 1], e_recv.at[j, 1], z_to(1)),
        )

    def mid_copy(i):
        j = column(i)
        return remote(sm.at[j, pl.ds(2, 2)], r_mid.at[j], m_send.at[j], m_recv.at[j], z_to(2))

    def fin_copy(i):
        j = column(i)
        return remote(sm.at[j, 1], r_fin.at[j], f_send.at[j], f_recv.at[j], z_to(1))

    def pair_sum(i):
        pair_copy(i).wait_recv()
        j = column(i)
        for k in range(4):
            sm[j, k] = add(part[j, plane[k], c], pc[j, plane[k]]).astype(jnp.bfloat16)
        start_end(end_copies(i)[0])

    def end_rest(*which):
        for i in which:
            start_end(end_copies(i)[1])

    def pass_on(i):
        j = column(i)
        end_copies(i)[0].wait_recv()
        sm[j, 2] = add(sm[j, 2], r_end[j, 1]).astype(jnp.bfloat16)
        sm[j, 3] = add(sm[j, 3], r_end[j, 2]).astype(jnp.bfloat16)
        mid_copy(i).start()

    def pass_early(i):
        pl.when(is_mid)(lambda: pass_on(i))

    def piece(i, tt):
        return out_ref.at[tt, :, pl.ds(pl.multiple_of(column(i) * cw, cw), cw)]

    def share_copies(i):
        j, own, other = column(i), piece(i, t), piece(i, (t + 2) % 4)
        return [
            remote(src, src, o_send.at[j, n], o_recv.at[j, n], to)
            for n, (src, to) in enumerate(((own, y_to), (own, c_to), (other, c_to)))
        ]

    def share(i):
        for copy in share_copies(i)[:2]:
            copy.start()

    def hand_back(i):
        j = column(i)
        mid_copy(i).wait_recv()
        sm[j, 1] = add(sm[j, 1], r_mid[j, 1]).astype(jnp.bfloat16)
        fin_copy(i).start()

    def finish_mid(i):
        j = column(i)
        at = pl.ds(pl.multiple_of(j * cw, cw), cw)
        end_copies(i)[1].wait_recv()
        out_ref[t, :, at] = add(sm[j, 0], r_end[j, 0], r_mid[j, 0]).astype(jnp.bfloat16)
        share(i)

    def finish_end(i):
        j = column(i)
        at = pl.ds(pl.multiple_of(j * cw, cw), cw)
        fin_copy(i).wait_recv()
        out_ref[t, :, at] = add(sm[j, 0], r_fin[j]).astype(jnp.bfloat16)
        share(i)

    def forward(i):
        copies = share_copies(i)
        copies[0].wait_recv()
        copies[2].start()

    spread(DOWN, 2)
    settle(DOWN, 0)
    settle(DOWN, 1)
    down_chunk(0)
    down_chunk(1)
    pair_sum(0)
    down_chunk(2)
    pair_sum(1)
    pair_sum(2)
    end_rest(0, 1, 2)
    relay(DOWN, 2)
    pass_early(0)
    spread(DOWN, 3)
    pass_early(1)
    settle(DOWN, 2)
    down_chunk(3)
    pair_sum(3)
    relay(DOWN, 3)
    pass_early(2)
    settle(DOWN, 3)
    down_chunk(4)
    down_chunk(5)
    pair_sum(4)
    pair_sum(5)
    end_rest(3, 4, 5)

    @pl.when(is_mid)
    def _():
        hand_back(3)
        pass_on(3)
        hand_back(4)
        hand_back(5)
        pass_on(4)
        hand_back(0)
        pass_on(5)
        finish_mid(0)
        hand_back(1)
        finish_mid(1)
        forward(0)
        finish_mid(3)
        forward(1)
        hand_back(2)
        finish_mid(2)
        finish_mid(4)
        forward(3)
        forward(2)
        finish_mid(5)
        forward(4)
        forward(5)

    @pl.when(is_end)
    def _():
        finish_end(3)
        finish_end(4)
        forward(3)
        finish_end(5)
        forward(4)
        finish_end(0)
        forward(5)
        finish_end(1)
        forward(0)
        finish_end(2)
        forward(1)
        forward(2)

    for i in range(chunks):
        for copy in share_copies(i)[1:]:
            copy.wait_recv()
        for copy in share_copies(i):
            copy.wait_send()

    for copy in sent:
        copy.wait_send()

    @pl.when(is_end)
    def _():
        for copy in sent_end:
            copy.wait_send()

    @pl.when(is_mid)
    def _():
        for copy in sent_mid:
            copy.wait_send()
        for i in range(chunks):
            mid_copy(i).wait_send()
            fin_copy(i).wait_send()


def fused(tokens, norm_gain, gate_weight, up_weight, down_weight, branch_gain):
    rows, d = tokens.shape
    n_tp, planes = 4, 4
    rq = rows // n_tp
    hidden = gate_weight.shape[1]
    width = 2 * (hidden // planes)
    chunks = 2 * SUB
    cw = d // chunks
    bf16, f32, dma = jnp.bfloat16, jnp.float32, pltpu.SemaphoreType.DMA
    hbm = pl.BlockSpec(memory_space=pl.ANY)
    vmem = pl.BlockSpec(memory_space=pltpu.VMEM)
    out = pl.pallas_call(
        kernel,
        out_shape=jax.ShapeDtypeStruct((n_tp, rq, d), bf16),
        in_specs=[hbm] * 4 + [vmem],
        out_specs=vmem,
        scratch_shapes=[
            pltpu.VMEM((rq, d), bf16),
            pltpu.VMEM((planes, 2, rq, d), bf16),
            pltpu.VMEM((d, width), bf16),
            pltpu.VMEM((d, width), bf16),
            pltpu.VMEM((d, width), bf16),
            pltpu.VMEM((planes, 2 * rq, width), f32),
            pltpu.VMEM((planes, 2 * rq, width), bf16),
            pltpu.VMEM((chunks, planes, 2, rq, cw), bf16),
            pltpu.VMEM((chunks, planes, rq, cw), bf16),
            pltpu.VMEM((chunks, planes, rq, cw), bf16),
            pltpu.VMEM((chunks, 3, rq, cw), bf16),
            pltpu.VMEM((chunks, 2, rq, cw), bf16),
            pltpu.VMEM((chunks, rq, cw), bf16),
            dma((4,)),
            dma((3, 4)), dma((3, 4)),
            dma((3, 4)), dma((3, 4)),
            dma((3, 4)), dma((3, 4)),
            dma((3, 4)), dma((3, 4)),
            dma((3, 4)), dma((3, 4)),
            dma((5, rq // STRIP)), dma((4, rq // STRIP)),
            dma((4,)), dma((4,)),
            dma((chunks,)), dma((chunks,)),
            dma((chunks, 2)), dma((chunks, 2)),
            dma((chunks,)), dma((chunks,)),
            dma((chunks,)), dma((chunks,)),
            dma((chunks, 3)), dma((chunks, 3)),
        ],
        compiler_params=pltpu.CompilerParams(
            collective_id=0, has_side_effects=True, vmem_limit_bytes=60 * 1024 * 1024
        ),
    )(
        tokens.reshape(n_tp, rq, d), gate_weight, up_weight, down_weight.T, norm_gain.reshape(1, d),
    )
    return complete(tokens, out.reshape(rows, d).astype(jnp.float32), branch_gain)


def solution(mesh):
    n_fs, n_tp = mesh.shape["fs"], mesh.shape["tp"]

    def per_device(*args):
        tokens, _, gate_weight = args[:3]
        rows, d = tokens.shape
        depth, hidden = gate_weight.shape
        fits = (
            n_fs == 8
            and n_tp == 4
            and rows % (STRIP * n_tp) == 0
            and depth % (2 * STRIP) == 0
            and hidden % (128 * 4) == 0
            and d % (128 * 2 * SUB) == 0
        )
        if fits:
            return fused(*args)
        return plain(*args)

    in_specs = (P("fs", None), P(), P("fs", "tp"), P("fs", "tp"), P("tp", "fs"), P())
    return jax.shard_map(
        per_device, mesh=mesh, in_specs=in_specs, out_specs=P("fs", None), check_vma=False
    )
```

time: 179 us -> 145 us (0.81)
  Pallas kernels: 171 us -> 137 us
    pallas_call x1, Pallas kernels: 171 us -> 137 us  [fused(): pl.pallas_call(kernel, out_shape=jax.ShapeDtypeStruct((n_tp, rq, d), bf16...]
where the time goes in v1:
time: 145 us
  Pallas kernels  137 us (94%)
  other arithmetic  6 us (4%)
    pallas_call x1, Pallas kernels, fused(): pl.pallas_call(kernel, out_shape=jax.ShapeDtypeStruct((n_tp, rq, d), bf16...  137 us
    convert_element_type x1, other arithmetic, complete(): (own_tokens.astype(jnp.float32) + summed * branch_scale * branch_gain).as...  3.78 us

profile of v1, /device:TPU:0, one launch (start us, length us, event | category | flops | bytes accessed | tf_op | source)
XLA Modules:
  0.0 144.9 jit_solution(3696620572086506346)
XLA Ops:
  0.0 1.3 reshape.28.gain_ref
  1.3 0.0 copy-start.1
  1.3 137.5 %shard_map.64 = bf16[4,112,2304]{2,1,0:T(8,128)(2,1)} custom-call(bf16[4,112,2304]{2,1,0:T(8,128)(2,1)} %bitcast.10, bf16[288,1536]{1,0:T(8,128)(2,1)} %gate_ref.1, bf16[288,1536]{1,0:T(8,128)(2,1)} %up_ref.1, bf16[288,1536]{1,0:T(8,128)(2,1)} %bitcast.11, f32[1,2304]{1,0:T(1,128)} %reshape.28.gain_ref), custom_call_target="tpu_custom_call" | custom-call | tf_op jit(solution)/shard_map/pallas_call | solution.py:480
  138.8 0.0 copy-start
  138.8 2.2 %multiply_reduce_fusion = f32[4,112]{1,0:T(4,128)S(1)} fusion(bf16[4,112,2304]{2,1,0:T(8,128)(2,1)} %shard_map.64), kind=kLoop, calls=%fused_computation.4 | loop fusion | flops 3096128 | bytes 2066176 | tf_op jit(solution)/shard_map/reduce_sum | solution.py:18
  141.0 0.1 rsqrt.12
  141.1 0.0 copy-done.1
  141.1 0.0 copy-done
  141.1 3.8 %fusion.2 = bf16[448,2304]{1,0:T(8,128)(2,1)} fusion(bf16[448,2304]{1,0:T(8,128)(2,1)} %param.6, f32[2304]{0:T(1024)S(1)} %copy-done.1, f32[448]{0:T(512)S(1)} %rsqrt.12, bf16[4,112,2304]{2,1,0:T(8,128)(2,1)S(1)} %copy-done), kind=kLoop, calls=%fused_computation.3 | loop fusion | flops 6193152 | bytes 6204160 | tf_op jit(solution)/shard_map/convert_element_type | solution.py:19
  (1 shorter events, 0.0 us)
Async XLA Ops:
  1.3 139.8 %copy-start.1 = (f32[2304]{0:T(1024)S(1)}, f32[2304]{0:T(1024)}, u32[]{:S(2)}) copy-start(f32[2304]{0:T(1024)} %param.11) | copy-start | bytes 27652
  138.8 2.3 %copy-start = (bf16[4,112,2304]{2,1,0:T(8,128)(2,1)S(1)}, bf16[4,112,2304]{2,1,0:T(8,128)(2,1)}, u32[]{:S(2)}) copy-start(bf16[4,112,2304]{2,1,0:T(8,128)(2,1)} %shard_map.64) | copy-start | bytes 6193156

commit v2 on v1

v2 whole, which is shorter than its diff:
```python
import functools

import jax
import jax.numpy as jnp
from jax import lax
from jax.experimental import pallas as pl
from jax.experimental.pallas import tpu as pltpu
from jax.sharding import PartitionSpec as P

MESH = pl.DeviceIdType.MESH
epsilon = 1e-06
GATE, UP, DOWN = 0, 1, 2
SUB = 3
STRIP = 16


def complete(own_tokens, summed, branch_gain):
    branch_scale = lax.rsqrt(jnp.mean(summed * summed, axis=-1, keepdims=True) + epsilon)
    return (own_tokens.astype(jnp.float32) + summed * branch_scale * branch_gain).astype(
        jnp.bfloat16
    )


def normalize(tokens, norm_gain):
    widened = tokens.astype(jnp.float32)
    scale = lax.rsqrt(jnp.mean(widened * widened, axis=-1, keepdims=True) + epsilon)
    return (widened * scale * norm_gain).astype(jnp.bfloat16)


def plain(tokens, norm_gain, gate_weight, up_weight, down_weight, branch_gain):
    normed = normalize(tokens, norm_gain)
    gate_whole, up_whole = (
        lax.all_gather(gate_weight, "fs", axis=0, tiled=True),
        lax.all_gather(up_weight, "fs", axis=0, tiled=True),
    )
    gate_sum = jnp.dot(normed, gate_whole, preferred_element_type=jnp.float32)
    up_sum = jnp.dot(normed, up_whole, preferred_element_type=jnp.float32)
    hidden = (jax.nn.silu(gate_sum) * up_sum).astype(jnp.bfloat16)
    partial_value = jnp.dot(
        hidden,
        lax.all_gather(down_weight, "fs", axis=1, tiled=True),
        preferred_element_type=jnp.float32,
    )
    summed = lax.psum(partial_value.astype(jnp.bfloat16), "tp").astype(jnp.float32)
    return complete(tokens, summed, branch_gain)


def kernel(tokens_ref, gate_ref, up_ref, down_ref, norm_gain_ref, branch_gain_ref, result_ref, *scratch):
    xs, gains, out_ref, xn, wg, wu, wd, gated, hid, part, pc, sm, r_end, r_mid, r_fin = scratch[:15]
    (loc_sem, z_send, z_recv, x_send, x_recv, y_send, y_recv, dx_send, dx_recv, dy_send, dy_recv,
     t_send, t_recv, td_send, td_recv, c_send, c_recv, e_send, e_recv, m_send, m_recv, f_send, f_recv,
     o_send, o_recv, w_sem) = scratch[15:]
    f, t = lax.axis_index("fs"), lax.axis_index("tp")
    z, x, y, c = f // 2, f % 2, t // 2, t % 2
    h = z // 2
    middling = (z % 2 + z // 2) % 2
    is_mid, is_end = middling == 1, middling == 0
    plane = [z, z + 1 - 2 * (z % 2), 2 - h, 3 - 3 * h]
    slot = [0, 1, 3 - middling, 3 - middling]
    depth, width = gate_ref.shape[0], wg.shape[1] // 2
    rq, d = xn.shape[2:]
    strips = rq // STRIP
    chunks, cw = part.shape[0], part.shape[-1]
    rows = 8 * rq
    weights, inputs = (wg, wu, wd), (gate_ref, up_ref, down_ref)

    x_to, y_to, c_to = (f + 1 - 2 * x, t), (f, (t + 2) % 4), (f, t + 1 - 2 * c)
    yc_to = (f, (1 - y) * 2 + 1 - c)

    def z_to(k):
        return (plane[k] * 2 + x, t)

    barrier = pltpu.get_barrier_semaphore()
    for peer in (x_to, y_to, c_to, yc_to, z_to(1), z_to(2), z_to(3)):
        pl.semaphore_signal(barrier, inc=1, device_id=peer, device_id_type=MESH)

    def remote(src, dst, send, recv, to):
        return pltpu.make_async_remote_copy(
            src, dst, send, recv, device_id=to, device_id_type=MESH
        )

    def block(a, k, yy, lo=0, n=depth, flip=0):
        ff = plane[k] * 2 + (1 - x if flip else x)
        at = pl.ds(pl.multiple_of(ff * depth + lo, STRIP), n)
        return weights[a].at[at, pl.ds(pl.multiple_of(yy * width, width), width)]

    def quarter(a, k):
        return inputs[a].at[:, pl.ds(pl.multiple_of(plane[k] * width, width), width)]

    early = [
        pltpu.make_async_copy(tokens_ref, xs, loc_sem.at[3]),
        pltpu.make_async_copy(norm_gain_ref, gains.at[0, 0], loc_sem.at[4]),
        pltpu.make_async_copy(branch_gain_ref, gains.at[1, 0], loc_sem.at[5]),
    ]
    local = early + [
        pltpu.make_async_copy(quarter(a, 0), block(a, 0, y), loc_sem.at[a]) for a in range(3)
    ]
    for copy in local:
        copy.start()

    def z_copy(a, k):
        return remote(
            quarter(a, k), block(a, 0, y), z_send.at[a, k], z_recv.at[a, slot[k]], z_to(k)
        )

    def z_wait(a, k):
        piece = block(a, k, y)
        remote(piece, piece, z_send.at[a, k], z_recv.at[a, k], z_to(k)).wait_recv()

    def across(a, k):
        src = quarter(a, 0) if k == 0 else block(a, k, y)
        return (
            remote(src, block(a, k, y), x_send.at[a, k], x_recv.at[a, k], x_to),
            remote(src, block(a, k, y), y_send.at[a, k], y_recv.at[a, k], y_to),
        )

    def diagonal(a, k):
        n = depth // 2
        first, second = block(a, k, y, 0, n, 1), block(a, k, 1 - y, n, n)
        return (
            remote(first, first, dy_send.at[a, k], dy_recv.at[a, k], y_to),
            remote(second, second, dx_send.at[a, k], dx_recv.at[a, k], x_to),
        )

    def spread(a, k):
        if k > 0:
            z_wait(a, k)
        for copy in across(a, k):
            copy.start()

    def relay(a, k):
        for got, on in zip(across(a, k), diagonal(a, k)):
            got.wait_recv()
            on.start()

    def settle(a, k):
        for got in diagonal(a, k):
            got.wait_recv()

    def strip(k, s):
        return xn.at[plane[k], c, pl.ds(s * STRIP, STRIP)]

    def token_copy(lane, k, s, to, slot):
        piece = strip(k, s)
        return remote(piece, piece, t_send.at[lane, s], t_recv.at[slot, s], to)

    def token_wait(k, s):
        token_copy(0, k, s, z_to(1), k).wait_recv()

    def token_pair(k):
        piece = xn.at[plane[k], c]
        return remote(piece, piece, td_send.at[k], td_recv.at[k], c_to)

    def token_lanes(mid):
        if mid:
            return [(0, 1, 1), (0, 2, 2), (1, 2, 3), (2, 1, 2), (3, 1, 3)]
        return [(0, 1, 1)]

    def token_relay(mid, lane, lo=0, hi=strips):
        k, to, there = token_lanes(mid)[lane]
        for s in range(lo, hi):
            if k > 0:
                token_wait(k, s)
            token_copy(lane, k, s, z_to(to), there).start()
        if k > 0 and hi == strips:
            token_pair(k).start()

    def token_take(k):
        for s in range(strips):
            token_wait(k, s)
        token_pair(k).start()

    def token_settle(*which):
        for k in which:
            token_pair(k).wait_recv()

    pl.semaphore_wait(barrier, 7)

    def sends(*pairs):
        for a, k in pairs:
            z_copy(a, k).start()

    @pl.when(is_end)
    def _():
        sends((GATE, 1), (GATE, 2), (GATE, 3), (UP, 1), (UP, 2), (UP, 3))

    @pl.when(is_mid)
    def _():
        sends((GATE, 2), (GATE, 1), (GATE, 3), (UP, 2), (UP, 1), (UP, 3))

    spread(GATE, 0)
    spread(UP, 0)

    for copy in early:
        copy.wait()
    for s in range(strips):
        at_rows = pl.ds(s * STRIP, STRIP)
        v = xs[t, at_rows, :].astype(jnp.float32)
        scale = lax.rsqrt(jnp.mean(v * v, axis=-1, keepdims=True) + epsilon)
        xn[z, c, at_rows, :] = (v * scale * gains[0]).astype(jnp.bfloat16)
    token_pair(0).start()

    @pl.when(is_end)
    def _():
        token_relay(False, 0)
        sends((DOWN, 1))

    @pl.when(is_mid)
    def _():
        token_relay(True, 1)
        token_relay(True, 0)

    def product(w, zb, nb, n0, nw):
        v = xn[pl.ds(zb, nb)].reshape(nb * 2 * rq, d)
        return jnp.dot(
            v, w[:, pl.ds(pl.multiple_of(n0, nw), nw)], preferred_element_type=jnp.float32
        )

    def gate_rows(zb, nb):
        def one(i, carry):
            n0 = pl.multiple_of(i * width, width)
            v = product(wg, zb, nb, n0, width)
            v = v / (1.0 + jnp.exp(-v))
            gated[pl.ds(zb, nb), :, pl.ds(n0, width)] = v.reshape(nb, 2 * rq, width)
            return carry

        lax.fori_loop(0, 2, one, 0)

    def up_rows(zb, nb):
        def one(i, carry):
            n0 = pl.multiple_of(i * width, width)
            v = product(wu, zb, nb, n0, width).reshape(nb, 2 * rq, width)
            v = gated[pl.ds(zb, nb), :, pl.ds(n0, width)] * v
            hid[pl.ds(zb, nb), :, pl.ds(n0, width)] = v.astype(jnp.bfloat16)
            return carry

        lax.fori_loop(0, 2, one, 0)

    def settle_all(a):
        for k in range(4):
            settle(a, k)

    def own_weights():
        for copy in local[3:]:
            copy.wait()

    @pl.when(is_end)
    def _():
        relay(GATE, 0)
        spread(GATE, 1)
        relay(UP, 0)
        spread(UP, 1)
        relay(GATE, 1)
        spread(GATE, 2)
        relay(UP, 1)
        spread(GATE, 3)
        relay(GATE, 2)
        spread(UP, 2)
        relay(GATE, 3)
        spread(UP, 3)
        relay(UP, 2)
        token_take(1)
        relay(UP, 3)
        spread(DOWN, 0)
        settle_all(GATE)
        own_weights()
        token_settle(0, 1)
        gate_rows(h * 2, 2)
        settle_all(UP)
        up_rows(h * 2, 2)
        sends((DOWN, 3), (DOWN, 2))
        token_take(2)
        relay(DOWN, 0)
        token_settle(2)
        gate_rows(plane[2], 1)
        up_rows(plane[2], 1)
        spread(DOWN, 1)
        token_take(3)
        token_settle(3)
        gate_rows(plane[3], 1)
        relay(DOWN, 1)
        up_rows(plane[3], 1)
        spread(DOWN, 2)
        settle(DOWN, 0)

    @pl.when(is_mid)
    def _():
        relay(GATE, 0)
        spread(GATE, 1)
        relay(UP, 0)
        spread(GATE, 2)
        relay(GATE, 1)
        spread(GATE, 3)
        spread(UP, 1)
        relay(GATE, 2)
        spread(UP, 2)
        relay(GATE, 3)
        relay(UP, 1)
        spread(UP, 3)
        sends((DOWN, 1))
        token_relay(True, 2)
        token_relay(True, 3, 0, 3)
        relay(UP, 2)
        token_relay(True, 3, 3)
        token_relay(True, 4, 0, 4)
        relay(UP, 3)
        spread(DOWN, 0)
        settle_all(GATE)
        own_weights()
        token_settle(0, 1)
        gate_rows(h * 2, 2)
        token_relay(True, 4, 4)
        sends((DOWN, 3), (DOWN, 2))
        settle_all(UP)
        up_rows(h * 2, 2)
        relay(DOWN, 0)
        spread(DOWN, 1)
        token_settle(2)
        gate_rows(plane[2], 1)
        up_rows(plane[2], 1)
        relay(DOWN, 1)
        token_settle(3)
        gate_rows(plane[3], 1)
        up_rows(plane[3], 1)
        settle(DOWN, 0)

    def column(i):
        return h * (chunks - 1) + (1 - 2 * h) * i

    def pair_copy(i):
        j = column(i)
        return remote(part.at[j, :, 1 - c], pc.at[j], c_send.at[j], c_recv.at[j], c_to)

    def down_chunk(i):
        j = column(i)
        value = lax.dot_general(
            hid[...].reshape(rows, 2 * width), wd[pl.ds(pl.multiple_of(j * cw, cw), cw), :], (((1,), (1,)), ((), ())),
            preferred_element_type=jnp.float32,
        ).astype(jnp.bfloat16)
        for zz in range(4):
            for cc in range(2):
                at = (zz * 2 + cc) * rq
                part[j, zz, cc] = value[at:at + rq]
        pair_copy(i).start()

    def add(*terms):
        return functools.reduce(lambda a, b: a + b, [v.astype(jnp.float32) for v in terms])

    first = (rq // STRIP + 1) // 2 * STRIP
    whole, halves = [(0, rq)], [(0, first), (first, rq - first)]

    def outward(i):
        return halves if i >= chunks - 2 else whole

    def inward(i):
        return halves if i < 2 else whole

    def end_copies(i):
        j = column(i)
        return [
            remote(
                sm.at[j, pl.ds(2, 2), pl.ds(lo, n)], r_end.at[j, pl.ds(1, 2), pl.ds(lo, n)],
                e_send.at[j, p], e_recv.at[j, p], z_to(1),
            )
            for p, (lo, n) in enumerate(outward(i))
        ]

    def end_copy(i):
        j = column(i)
        return remote(sm.at[j, 1], r_end.at[j, 0], e_send.at[j, 2], e_recv.at[j, 2], z_to(1))

    def mid_copies(i, parts):
        j = column(i)
        return [
            remote(
                sm.at[j, pl.ds(2, 2), pl.ds(lo, n)], r_mid.at[j, :, pl.ds(lo, n)],
                m_send.at[j, p], m_recv.at[j, p], z_to(2),
            )
            for p, (lo, n) in enumerate(parts)
        ]

    def fin_copies(i):
        j = column(i)
        return [
            remote(
                sm.at[j, 1, pl.ds(lo, n)], r_fin.at[j, pl.ds(lo, n)],
                f_send.at[j, p], f_recv.at[j, p], z_to(1),
            )
            for p, (lo, n) in enumerate(inward(i))
        ]

    def pair_sum(i):
        pair_copy(i).wait_recv()
        j = column(i)
        for k in range(4):
            sm[j, k] = add(part[j, plane[k], c], pc[j, plane[k]]).astype(jnp.bfloat16)

        @pl.when(is_end)
        def _():
            for copy in end_copies(i):
                copy.start()

    def end_rest(*which):
        for i in which:
            end_copy(i).start()

    def pass_on(i):
        j = column(i)
        for (lo, n), got, on in zip(outward(i), end_copies(i), mid_copies(i, outward(i))):
            at = pl.ds(lo, n)
            got.wait_recv()
            sm[j, 2, at] = add(sm[j, 2, at], r_end[j, 1, at]).astype(jnp.bfloat16)
            sm[j, 3, at] = add(sm[j, 3, at], r_end[j, 2, at]).astype(jnp.bfloat16)
            on.start()

    def share_copies(i):
        j = column(i)
        lanes = pl.ds(pl.multiple_of(j * cw, cw), cw)
        every = []
        for p, (lo, n) in enumerate(inward(i)):
            own, other = out_ref.at[t, pl.ds(lo, n), lanes], out_ref.at[(t + 2) % 4, pl.ds(lo, n), lanes]
            every.append([
                remote(src, src, o_send.at[j, 3 * p + k], o_recv.at[j, 3 * p + k], to)
                for k, (src, to) in enumerate(((own, y_to), (own, c_to), (other, c_to)))
            ])
        return every

    def share(i, p):
        for copy in share_copies(i)[p][:2]:
            copy.start()

    def hand_back(i):
        j = column(i)
        for (lo, n), got, on in zip(inward(i), mid_copies(i, inward(i)), fin_copies(i)):
            at = pl.ds(lo, n)
            got.wait_recv()
            sm[j, 1, at] = add(sm[j, 1, at], r_mid[j, 1, at]).astype(jnp.bfloat16)
            on.start()

    def finish_mid(i):
        j = column(i)
        lanes = pl.ds(pl.multiple_of(j * cw, cw), cw)
        end_copy(i).wait_recv()
        for p, (lo, n) in enumerate(inward(i)):
            at = pl.ds(lo, n)
            out_ref[t, at, lanes] = add(sm[j, 0, at], r_end[j, 0, at], r_mid[j, 0, at]).astype(jnp.bfloat16)
            share(i, p)

    def finish_end(i):
        j = column(i)
        lanes = pl.ds(pl.multiple_of(j * cw, cw), cw)
        for p, ((lo, n), got) in enumerate(zip(inward(i), fin_copies(i))):
            at = pl.ds(lo, n)
            got.wait_recv()
            out_ref[t, at, lanes] = add(sm[j, 0, at], r_fin[j, at]).astype(jnp.bfloat16)
            share(i, p)

    def forward(i):
        for copies in share_copies(i):
            copies[0].wait_recv()
            copies[2].start()

    @pl.when(is_end)
    def _():
        down_chunk(0)
        settle(DOWN, 1)
        pair_sum(0)
        down_chunk(1)
        down_chunk(2)
        pair_sum(1)
        spread(DOWN, 3)
        pair_sum(2)
        end_rest(2)
        relay(DOWN, 2)
        settle(DOWN, 2)
        down_chunk(3)
        pair_sum(3)
        end_rest(3)
        relay(DOWN, 3)
        settle(DOWN, 3)
        down_chunk(4)
        down_chunk(5)
        pair_sum(4)
        pair_sum(5)

    @pl.when(is_mid)
    def _():
        settle(DOWN, 1)
        down_chunk(0)
        down_chunk(1)
        pair_sum(0)
        down_chunk(2)
        pair_sum(1)
        pair_sum(2)
        spread(DOWN, 2)
        spread(DOWN, 3)
        relay(DOWN, 2)
        pass_on(0)
        pass_on(1)
        relay(DOWN, 3)
        settle(DOWN, 2)
        down_chunk(3)
        pair_sum(3)
        pass_on(2)
        settle(DOWN, 3)
        down_chunk(4)
        down_chunk(5)
        pair_sum(4)
        pair_sum(5)

    def weights_sent(a):
        for k in range(4):
            if k > 0:
                z_copy(a, k).wait_send()
            for copy in across(a, k) + diagonal(a, k):
                copy.wait_send()

    def tokens_sent(mid):
        for k in range(4):
            token_pair(k).wait_send()
        for lane, (k, to, there) in enumerate(token_lanes(mid)):
            for s in range(strips):
                token_copy(lane, k, s, z_to(to), there).wait_send()

    def pairs_sent():
        for i in range(chunks):
            pair_copy(i).wait_send()

    @pl.when(is_mid)
    def _():
        hand_back(5)
        hand_back(4)
        pass_on(3)
        hand_back(3)
        finish_mid(3)
        weights_sent(GATE)
        pass_on(4)
        hand_back(2)
        finish_mid(2)
        pass_on(5)
        forward(3)
        hand_back(1)
        finish_mid(4)
        finish_mid(5)
        hand_back(0)
        forward(2)
        finish_mid(1)
        finish_mid(0)
        weights_sent(UP)
        weights_sent(DOWN)
        forward(4)
        tokens_sent(True)
        forward(5)
        pairs_sent()
        forward(1)
        forward(0)

    @pl.when(is_end)
    def _():
        end_rest(4, 5, 1, 0)
        finish_end(5)
        finish_end(4)
        weights_sent(GATE)
        forward(5)
        finish_end(3)
        forward(4)
        weights_sent(UP)
        weights_sent(DOWN)
        finish_end(2)
        forward(3)
        tokens_sent(False)
        finish_end(1)
        forward(2)
        pairs_sent()
        finish_end(0)
        forward(1)
        forward(0)

    def written(tt):
        return pltpu.make_async_copy(xs.at[tt], result_ref.at[tt], w_sem.at[tt])

    def complete_piece(tt):
        v = out_ref[tt].astype(jnp.float32)
        scale = lax.rsqrt(jnp.mean(v * v, axis=-1, keepdims=True) + epsilon)
        xs[tt] = (xs[tt].astype(jnp.float32) + v * scale * gains[1]).astype(jnp.bfloat16)
        written(tt).start()

    def take_shares(n):
        for i in range(chunks):
            for copies in share_copies(i):
                copies[n].wait_recv()

    complete_piece(t)
    complete_piece((t + 2) % 4)
    for n in (1, 2):
        take_shares(n)
        complete_piece((t + 1 - 2 * c + 2 * (n - 1)) % 4)
    for tt in range(4):
        written(tt).wait()
    for i in range(chunks):
        for copies in share_copies(i):
            for copy in copies:
                copy.wait_send()

    @pl.when(is_end)
    def _():
        for i in range(chunks):
            for copy in end_copies(i) + [end_copy(i)]:
                copy.wait_send()

    @pl.when(is_mid)
    def _():
        for i in range(chunks):
            for copy in mid_copies(i, outward(i)) + fin_copies(i):
                copy.wait_send()


def fused(tokens, norm_gain, gate_weight, up_weight, down_weight, branch_gain):
    rows, d = tokens.shape
    n_tp, planes = 4, 4
    rq = rows // n_tp
    hidden = gate_weight.shape[1]
    width = 2 * (hidden // planes)
    chunks = 2 * SUB
    cw = d // chunks
    bf16, f32, dma = jnp.bfloat16, jnp.float32, pltpu.SemaphoreType.DMA
    hbm = pl.BlockSpec(memory_space=pl.ANY)
    out = pl.pallas_call(
        kernel,
        out_shape=jax.ShapeDtypeStruct((n_tp, rq, d), bf16),
        in_specs=[hbm] * 6,
        out_specs=hbm,
        scratch_shapes=[
            pltpu.VMEM((n_tp, rq, d), bf16),
            pltpu.VMEM((2, 1, d), f32),
            pltpu.VMEM((n_tp, rq, d), bf16),
            pltpu.VMEM((planes, 2, rq, d), bf16),
            pltpu.VMEM((d, width), bf16),
            pltpu.VMEM((d, width), bf16),
            pltpu.VMEM((d, width), bf16),
            pltpu.VMEM((planes, 2 * rq, width), f32),
            pltpu.VMEM((planes, 2 * rq, width), bf16),
            pltpu.VMEM((chunks, planes, 2, rq, cw), bf16),
            pltpu.VMEM((chunks, planes, rq, cw), bf16),
            pltpu.VMEM((chunks, planes, rq, cw), bf16),
            pltpu.VMEM((chunks, 3, rq, cw), bf16),
            pltpu.VMEM((chunks, 2, rq, cw), bf16),
            pltpu.VMEM((chunks, rq, cw), bf16),
            dma((6,)),
            dma((3, 4)), dma((3, 4)),
            dma((3, 4)), dma((3, 4)),
            dma((3, 4)), dma((3, 4)),
            dma((3, 4)), dma((3, 4)),
            dma((3, 4)), dma((3, 4)),
            dma((5, rq // STRIP)), dma((4, rq // STRIP)),
            dma((4,)), dma((4,)),
            dma((chunks,)), dma((chunks,)),
            dma((chunks, 3)), dma((chunks, 3)),
            dma((chunks, 2)), dma((chunks, 2)),
            dma((chunks, 2)), dma((chunks, 2)),
            dma((chunks, 6)), dma((chunks, 6)),
            dma((n_tp,)),
        ],
        compiler_params=pltpu.CompilerParams(
            collective_id=0, has_side_effects=True, vmem_limit_bytes=60 * 1024 * 1024
        ),
    )(
        tokens.reshape(n_tp, rq, d), gate_weight, up_weight, down_weight.T, norm_gain, branch_gain,
    )
    return out.reshape(rows, d)


def solution(mesh):
    n_fs, n_tp = mesh.shape["fs"], mesh.shape["tp"]

    def per_device(*args):
        tokens, _, gate_weight = args[:3]
        rows, d = tokens.shape
        depth, hidden = gate_weight.shape
        fits = (
            n_fs == 8
            and n_tp == 4
            and rows % (STRIP * n_tp) == 0
            and depth % (2 * STRIP) == 0
            and hidden % (128 * 4) == 0
            and d % (128 * 2 * SUB) == 0
        )
        if fits:
            return fused(*args)
        return plain(*args)

    in_specs = (P("fs", None), P(), P("fs", "tp"), P("fs", "tp"), P("tp", "fs"), P())
    return jax.shard_map(
        per_device, mesh=mesh, in_specs=in_specs, out_specs=P("fs", None), check_vma=False
    )
```

time: 145 us -> 139 us (0.959)
  other arithmetic: 6 us -> 0 us
  local copies, waits for them, and re-layouts: 1.41 us -> 3.02 us
    convert_element_type x1 -> x0, other arithmetic: 3.78 us -> none  [complete(): (own_tokens.astype(jnp.float32) + summed * branch_scale * branch_gain).as...]
    unnamed x4 -> x1, local copies, waits for them, and re-layouts: 0.01 us -> 3.02 us
    reduce_sum x1 -> x0, other arithmetic: 2.21 us -> none  [complete(): jnp.mean(summed * summed, axis=-1, keepdims=True) + epsilon]
where the time goes in v2:
time: 139 us
  Pallas kernels  136 us (98%)
  local copies, waits for them, and re-layouts  3.02 us (2%)
    pallas_call x1, Pallas kernels, fused(): pl.pallas_call(kernel, out_shape=jax.ShapeDtypeStruct((n_tp, rq, d), bf16...  136 us
    unnamed x1, local copies, waits for them, and re-layouts  3.02 us

profile of v2, /device:TPU:0, one launch (start us, length us, event | category | flops | bytes accessed | tf_op | source)
XLA Modules:
  0.0 139.1 jit_solution(13585485266384734754)
XLA Ops:
  0.0 136.0 %shard_map.64 = bf16[4,112,2304]{2,1,0:T(8,128)(2,1)} custom-call(bf16[4,112,2304]{2,1,0:T(8,128)(2,1)} %bitcast.4, bf16[288,1536]{1,0:T(8,128)(2,1)} %gate_ref.1, bf16[288,1536]{1,0:T(8,128)(2,1)} %up_ref.1, bf16[288,1536]{1,0:T(8,128)(2,1)} %bitcast.5, f32[2304]{0:T(1024)} %norm_gain_ref.1, f32[2304]{0:T(1024)} %branch_gain_ref.1), custom_call_target="tpu_custom_call" | custom-call | tf_op jit(solution)/shard_map/pallas_call | solution.py:628
  136.0 3.0 %copy.8 = bf16[448,2304]{1,0:T(8,128)(2,1)} copy(bf16[448,2304]{1,0:T(8,128)(2,1)} %bitcast.3) | data formatting | bytes 4128768

commit v3 on v2

--- a/solution.py
+++ b/solution.py
@@ -47,9 +47,8 @@
 
 def kernel(tokens_ref, gate_ref, up_ref, down_ref, norm_gain_ref, branch_gain_ref, result_ref, *scratch):
     xs, gains, out_ref, xn, wg, wu, wd, gated, hid, part, pc, sm, r_end, r_mid, r_fin = scratch[:15]
-    (loc_sem, z_send, z_recv, x_send, x_recv, y_send, y_recv, dx_send, dx_recv, dy_send, dy_recv,
-     t_send, t_recv, td_send, td_recv, c_send, c_recv, e_send, e_recv, m_send, m_recv, f_send, f_recv,
-     o_send, o_recv, w_sem) = scratch[15:]
+    (loc_sem, sends_sem, w_send, t_send, z_recv, s_recv, d_recv, t_recv, td_recv, c_recv, e_recv, m_recv,
+     f_recv, o_recv, oc_recv) = scratch[15:]
     f, t = lax.axis_index("fs"), lax.axis_index("tp")
     z, x, y, c = f // 2, f % 2, t // 2, t % 2
     h = z // 2
@@ -98,28 +97,38 @@
     for copy in local:
         copy.start()
 
+    td_send, c_send, e_send, m_send, f_send, o_send, w_sem = (sends_sem.at[i] for i in range(7))
+
+    def stretch(a, n):
+        return weights[a].at[pl.ds(0, n * depth), pl.ds(0, width)]
+
+    def wait_sent(piece, sem):
+        remote(piece, piece, sem, oc_recv.at[0], c_to).wait_send()
+
+    def wait_got(piece, sem):
+        remote(piece, piece, w_sem, sem, c_to).wait_recv()
+
     def z_copy(a, k):
         return remote(
-            quarter(a, k), block(a, 0, y), z_send.at[a, k], z_recv.at[a, slot[k]], z_to(k)
+            quarter(a, k), block(a, 0, y), w_send.at[a, 0], z_recv.at[a, slot[k]], z_to(k)
         )
 
     def z_wait(a, k):
-        piece = block(a, k, y)
-        remote(piece, piece, z_send.at[a, k], z_recv.at[a, k], z_to(k)).wait_recv()
+        wait_got(stretch(a, 1), z_recv.at[a, k])
 
     def across(a, k):
         src = quarter(a, 0) if k == 0 else block(a, k, y)
         return (
-            remote(src, block(a, k, y), x_send.at[a, k], x_recv.at[a, k], x_to),
-            remote(src, block(a, k, y), y_send.at[a, k], y_recv.at[a, k], y_to),
+            remote(src, block(a, k, y), w_send.at[a, 1], s_recv.at[a, k], x_to),
+            remote(src, block(a, k, y), w_send.at[a, 1], s_recv.at[a, k], y_to),
         )
 
     def diagonal(a, k):
         n = depth // 2
         first, second = block(a, k, y, 0, n, 1), block(a, k, 1 - y, n, n)
         return (
-            remote(first, first, dy_send.at[a, k], dy_recv.at[a, k], y_to),
-            remote(second, second, dx_send.at[a, k], dx_recv.at[a, k], x_to),
+            remote(first, first, w_send.at[a, 2], d_recv.at[a, k], y_to),
+            remote(second, second, w_send.at[a, 2], d_recv.at[a, k], x_to),
         )
 
     def spread(a, k):
@@ -129,27 +138,26 @@
             copy.start()
 
     def relay(a, k):
-        for got, on in zip(across(a, k), diagonal(a, k)):
-            got.wait_recv()
-            on.start()
+        wait_got(stretch(a, 2), s_recv.at[a, k])
+        for copy in diagonal(a, k):
+            copy.start()
 
     def settle(a, k):
-        for got in diagonal(a, k):
-            got.wait_recv()
+        wait_got(stretch(a, 1), d_recv.at[a, k])
 
     def strip(k, s):
         return xn.at[plane[k], c, pl.ds(s * STRIP, STRIP)]
 
     def token_copy(lane, k, s, to, slot):
         piece = strip(k, s)
-        return remote(piece, piece, t_send.at[lane, s], t_recv.at[slot, s], to)
+        return remote(piece, piece, t_send.at[lane], t_recv.at[slot - 1, s], to)
 
     def token_wait(k, s):
-        token_copy(0, k, s, z_to(1), k).wait_recv()
+        wait_got(strip(k, s), t_recv.at[k - 1, s])
 
     def token_pair(k):
         piece = xn.at[plane[k], c]
-        return remote(piece, piece, td_send.at[k], td_recv.at[k], c_to)
+        return remote(piece, piece, td_send, td_recv.at[k], c_to)
 
     def token_lanes(mid):
         if mid:
@@ -172,7 +180,7 @@
 
     def token_settle(*which):
         for k in which:
-            token_pair(k).wait_recv()
+            wait_got(xn.at[0, 0], td_recv.at[k])
 
     pl.semaphore_wait(barrier, 7)
 
@@ -329,7 +337,7 @@
 
     def pair_copy(i):
         j = column(i)
-        return remote(part.at[j, :, 1 - c], pc.at[j], c_send.at[j], c_recv.at[j], c_to)
+        return remote(part.at[j, :, 1 - c], pc.at[j], c_send, c_recv.at[j], c_to)
 
     def down_chunk(i):
         j = column(i)
@@ -360,21 +368,21 @@
         return [
             remote(
                 sm.at[j, pl.ds(2, 2), pl.ds(lo, n)], r_end.at[j, pl.ds(1, 2), pl.ds(lo, n)],
-                e_send.at[j, p], e_recv.at[j, p], z_to(1),
+                e_send, e_recv.at[j, p], z_to(1),
             )
             for p, (lo, n) in enumerate(outward(i))
         ]
 
     def end_copy(i):
         j = column(i)
-        return remote(sm.at[j, 1], r_end.at[j, 0], e_send.at[j, 2], e_recv.at[j, 2], z_to(1))
+        return remote(sm.at[j, 1], r_end.at[j, 0], e_send, e_recv.at[j, 2], z_to(1))
 
     def mid_copies(i, parts):
         j = column(i)
         return [
             remote(
                 sm.at[j, pl.ds(2, 2), pl.ds(lo, n)], r_mid.at[j, :, pl.ds(lo, n)],
-                m_send.at[j, p], m_recv.at[j, p], z_to(2),
+                m_send, m_recv.at[j, p], z_to(2),
             )
             for p, (lo, n) in enumerate(parts)
         ]
@@ -384,7 +392,7 @@
         return [
             remote(
                 sm.at[j, 1, pl.ds(lo, n)], r_fin.at[j, pl.ds(lo, n)],
-                f_send.at[j, p], f_recv.at[j, p], z_to(1),
+                f_send, f_recv.at[j, p], z_to(1),
             )
             for p, (lo, n) in enumerate(inward(i))
         ]
@@ -420,8 +428,9 @@
         for p, (lo, n) in enumerate(inward(i)):
             own, other = out_ref.at[t, pl.ds(lo, n), lanes], out_ref.at[(t + 2) % 4, pl.ds(lo, n), lanes]
             every.append([
-                remote(src, src, o_send.at[j, 3 * p + k], o_recv.at[j, 3 * p + k], to)
-                for k, (src, to) in enumerate(((own, y_to), (own, c_to), (other, c_to)))
+                remote(own, own, o_send, o_recv.at[j, p], y_to),
+                remote(own, own, o_send, oc_recv.at[0], c_to),
+                remote(other, other, o_send, oc_recv.at[1], c_to),
             ])
         return every
 
@@ -509,22 +518,17 @@
         pair_sum(5)
 
     def weights_sent(a):
-        for k in range(4):
-            if k > 0:
-                z_copy(a, k).wait_send()
-            for copy in across(a, k) + diagonal(a, k):
-                copy.wait_send()
+        wait_sent(stretch(a, 3), w_send.at[a, 0])
+        wait_sent(stretch(a, 8), w_send.at[a, 1])
+        wait_sent(stretch(a, 4), w_send.at[a, 2])
 
     def tokens_sent(mid):
-        for k in range(4):
-            token_pair(k).wait_send()
-        for lane, (k, to, there) in enumerate(token_lanes(mid)):
-            for s in range(strips):
-                token_copy(lane, k, s, z_to(to), there).wait_send()
+        wait_sent(xn.at[:, 0], td_send)
+        for lane in range(len(token_lanes(mid))):
+            wait_sent(xn.at[0, 0], t_send.at[lane])
 
     def pairs_sent():
-        for i in range(chunks):
-            pair_copy(i).wait_send()
+        wait_sent(pc, c_send)
 
     @pl.when(is_mid)
     def _():
@@ -576,43 +580,29 @@
         forward(1)
         forward(0)
 
-    def written(tt):
-        return pltpu.make_async_copy(xs.at[tt], result_ref.at[tt], w_sem.at[tt])
-
     def complete_piece(tt):
         v = out_ref[tt].astype(jnp.float32)
         scale = lax.rsqrt(jnp.mean(v * v, axis=-1, keepdims=True) + epsilon)
         xs[tt] = (xs[tt].astype(jnp.float32) + v * scale * gains[1]).astype(jnp.bfloat16)
-        written(tt).start()
-
-    def take_shares(n):
-        for i in range(chunks):
-            for copies in share_copies(i):
-                copies[n].wait_recv()
+        pltpu.make_async_copy(xs.at[tt], result_ref.at[tt], w_sem).start()
 
     complete_piece(t)
     complete_piece((t + 2) % 4)
-    for n in (1, 2):
-        take_shares(n)
-        complete_piece((t + 1 - 2 * c + 2 * (n - 1)) % 4)
-    for tt in range(4):
-        written(tt).wait()
-    for i in range(chunks):
-        for copies in share_copies(i):
-            for copy in copies:
-                copy.wait_send()
+    for n in range(2):
+        wait_got(out_ref.at[0], oc_recv.at[n])
+        complete_piece((t + 1 - 2 * c + 2 * n) % 4)
+    wait_sent(out_ref.at[pl.ds(0, 3)], o_send)
 
     @pl.when(is_end)
     def _():
-        for i in range(chunks):
-            for copy in end_copies(i) + [end_copy(i)]:
-                copy.wait_send()
+        wait_sent(r_end, e_send)
 
     @pl.when(is_mid)
     def _():
-        for i in range(chunks):
-            for copy in mid_copies(i, outward(i)) + fin_copies(i):
-                copy.wait_send()
+        wait_sent(r_mid, m_send)
+        wait_sent(r_fin, f_send)
+
+    pltpu.make_async_copy(xs, result_ref, w_sem).wait()
 
 
 def fused(tokens, norm_gain, gate_weight, up_weight, down_weight, branch_gain):
@@ -646,20 +636,10 @@
             pltpu.VMEM((chunks, 3, rq, cw), bf16),
             pltpu.VMEM((chunks, 2, rq, cw), bf16),
             pltpu.VMEM((chunks, rq, cw), bf16),
-            dma((6,)),
-            dma((3, 4)), dma((3, 4)),
-            dma((3, 4)), dma((3, 4)),
-            dma((3, 4)), dma((3, 4)),
-            dma((3, 4)), dma((3, 4)),
-            dma((3, 4)), dma((3, 4)),
-            dma((5, rq // STRIP)), dma((4, rq // STRIP)),
-            dma((4,)), dma((4,)),
-            dma((chunks,)), dma((chunks,)),
-            dma((chunks, 3)), dma((chunks, 3)),
-            dma((chunks, 2)), dma((chunks, 2)),
-            dma((chunks, 2)), dma((chunks, 2)),
-            dma((chunks, 6)), dma((chunks, 6)),
-            dma((n_tp,)),
+            dma((6,)), dma((7,)), dma((3, 3)), dma((5,)),
+            dma((3, 4)), dma((3, 4)), dma((3, 4)),
+            dma((3, rq // STRIP)), dma((4,)), dma((chunks,)),
+            dma((chunks, 3)), dma((chunks, 2)), dma((chunks, 2)), dma((chunks, 2)), dma((2,)),
         ],
         compiler_params=pltpu.CompilerParams(
             collective_id=0, has_side_effects=True, vmem_limit_bytes=60 * 1024 * 1024

time: 139 us -> 137 us (0.986)
  Pallas kernels: 136 us -> 134 us
    pallas_call x1, Pallas kernels: 136 us -> 134 us  [fused(): pl.pallas_call(kernel, out_shape=jax.ShapeDtypeStruct((n_tp, rq, d), bf16...]
where the time goes in v3:
time: 137 us
  Pallas kernels  134 us (98%)
  local copies, waits for them, and re-layouts  3.02 us (2%)
    pallas_call x1, Pallas kernels, fused(): pl.pallas_call(kernel, out_shape=jax.ShapeDtypeStruct((n_tp, rq, d), bf16...  134 us
    unnamed x1, local copies, waits for them, and re-layouts  3.02 us

profile of v3, /device:TPU:0, one launch (start us, length us, event | category | flops | bytes accessed | tf_op | source)
XLA Modules:
  0.0 137.0 jit_solution(10581523798866754266)
XLA Ops:
  0.0 134.0 %shard_map.64 = bf16[4,112,2304]{2,1,0:T(8,128)(2,1)} custom-call(bf16[4,112,2304]{2,1,0:T(8,128)(2,1)} %bitcast.4, bf16[288,1536]{1,0:T(8,128)(2,1)} %gate_ref.1, bf16[288,1536]{1,0:T(8,128)(2,1)} %up_ref.1, bf16[288,1536]{1,0:T(8,128)(2,1)} %bitcast.5, f32[2304]{0:T(1024)} %norm_gain_ref.1, f32[2304]{0:T(1024)} %branch_gain_ref.1), custom_call_target="tpu_custom_call" | custom-call | tf_op jit(solution)/shard_map/pallas_call | solution.py:618
  134.0 3.0 %copy.8 = bf16[448,2304]{1,0:T(8,128)(2,1)} copy(bf16[448,2304]{1,0:T(8,128)(2,1)} %bitcast.3) | data formatting | bytes 4128768

commit v4 on v3

--- a/solution.py
+++ b/solution.py
@@ -472,15 +472,15 @@
     @pl.when(is_end)
     def _():
         down_chunk(0)
+        pair_sum(0)
         settle(DOWN, 1)
-        pair_sum(0)
+        relay(DOWN, 2)
+        spread(DOWN, 3)
         down_chunk(1)
         down_chunk(2)
         pair_sum(1)
-        spread(DOWN, 3)
         pair_sum(2)
         end_rest(2)
-        relay(DOWN, 2)
         settle(DOWN, 2)
         down_chunk(3)
         pair_sum(3)

time: 137 us -> 138 us (level)
  no operation moved by 1% of the time
where the time goes in v4:
time: 138 us
  Pallas kernels  135 us (98%)
  local copies, waits for them, and re-layouts  3.02 us (2%)
    pallas_call x1, Pallas kernels, fused(): pl.pallas_call(kernel, out_shape=jax.ShapeDtypeStruct((n_tp, rq, d), bf16...  135 us
    unnamed x1, local copies, waits for them, and re-layouts  3.02 us

profile of v4, /device:TPU:0, one launch (start us, length us, event | category | flops | bytes accessed | tf_op | source)
XLA Modules:
  0.0 138.1 jit_solution(6650438376821281303)
XLA Ops:
  0.0 135.1 %shard_map.64 = bf16[4,112,2304]{2,1,0:T(8,128)(2,1)} custom-call(bf16[4,112,2304]{2,1,0:T(8,128)(2,1)} %bitcast.4, bf16[288,1536]{1,0:T(8,128)(2,1)} %gate_ref.1, bf16[288,1536]{1,0:T(8,128)(2,1)} %up_ref.1, bf16[288,1536]{1,0:T(8,128)(2,1)} %bitcast.5, f32[2304]{0:T(1024)} %norm_gain_ref.1, f32[2304]{0:T(1024)} %branch_gain_ref.1), custom_call_target="tpu_custom_call" | custom-call | tf_op jit(solution)/shard_map/pallas_call | solution.py:618
  135.1 3.0 %copy.8 = bf16[448,2304]{1,0:T(8,128)(2,1)} copy(bf16[448,2304]{1,0:T(8,128)(2,1)} %bitcast.3) | data formatting | bytes 4128768
